TPU v7x, 32 devices: a whole 2x2x4 slice. The times are simulated.
32 devices in a mesh: grp: 2 (over y), sp: 4 (over z), tp: 4 (over x, core).
Axes of the slice: x: 2, y: 2, z: 4, core: 2. Of those that a mesh axis runs over, the one named last changes fastest.
Arguments:
- query_a: bfloat16 [2048, 2048], P(('grp', 'sp'), 'tp'), parts along dimension 0, may hold values from -6 to 6
- key_a: bfloat16 [2048, 2048], P(('grp', 'sp'), 'tp'), parts along dimension 0, may hold values from -6 to 6
- value_a: bfloat16 [2048, 4096], P(('grp', 'sp'), 'tp'), parts along dimension 0, may hold values from -6 to 6
- decay_a: float32 [2, 8, 2048], P(None, 'tp', ('grp', 'sp')), parts along dimension 2, may hold values from -1 to 0
- query_b: bfloat16 [2048, 1024], P(('grp', 'sp'), 'tp'), parts along dimension 0, may hold values from -6 to 6
- key_b: bfloat16 [2048, 1024], P(('grp', 'sp'), 'tp'), parts along dimension 0, may hold values from -6 to 6
- value_b: bfloat16 [2048, 1024], P(('grp', 'sp'), 'tp'), parts along dimension 0, may hold values from -6 to 6
- decay_b: float32 [2, 16, 2048], P(None, 'tp', ('grp', 'sp')), parts along dimension 2, may hold values from -1 to 0
- out_weight_a: bfloat16 [4096, 2048], P('tp'), may hold values from -0.078125 to 0.078125
- out_weight_b: bfloat16 [1024, 2048], P('tp'), may hold values from -0.078125 to 0.078125
- residual: bfloat16 [2048, 2048], P(('grp', 'sp', 'tp')), parts along dimension 0, may hold values from -6 to 6
- norm_gain: float32 [2, 2048], replicated, may hold values from 0.1 to 1.9
- route_group: int32 [2048], P(('grp', 'sp', 'tp')), parts along dimension 0, may hold values from 0 to 3
- route_expert: int32 [2048, 2], P(('grp', 'sp', 'tp')), parts along dimension 0, may hold values from 0 to 7, as said below
- route_weight: float32 [2048, 2], P(('grp', 'sp', 'tp')), parts along dimension 0, may hold values from 0.2 to 1
- expert_gate: bfloat16 [32, 2048, 1024], P('sp', None, 'tp'), may hold values from -0.125 to 0.125
- expert_up: bfloat16 [32, 2048, 1024], P('sp', None, 'tp'), may hold values from -0.125 to 0.125
- expert_down: bfloat16 [32, 1024, 2048], P('sp', 'tp'), may hold values from -0.1875 to 0.1875
Outputs:
- layer_out: bfloat16 [2048, 2048], P(('grp', 'sp', 'tp')), parts along dimension 0
There are 2 independent parts, one for each index of `grp`. A program takes and returns all parts, laid end to end along the dimension named above; an argument that names none is the same for every part. Nothing has to cross between parts.
Inputs may be any that keep to these rules, and one draw needn't show every extreme that they name: `route_expert`: the 2 entries of a row are different.
All inputs are finite; a program needn't handle non-finite values.
Results may differ from a plain program's by a relative error of at most 0.015.
Values may be sent and summed in bfloat16 or wider, within the bound.
A program may use at most 128 MiB of HBM per device.

v0:
```python
import math

import jax
import jax.numpy as jnp
from jax import lax
from jax.sharding import PartitionSpec as P

BLOCK = 128
EXPERTS = 32
TOP = 2
CAP = 2
EXP_GROUP = 8


HIGHEST = lax.Precision.HIGHEST
RESIDUAL_SCALE = math.sqrt(2.0)
NORM_EPS = 1e-05
GROUP_EPS = 1e-06
ROPE_BASE = 10000.0


def entering(array, axis, join, neutral, backward):
    count = lax.axis_size(axis)
    place = lax.axis_index(axis)
    ahead = count - 1 - place if backward else place
    gathered = jax.tree.map(
        lambda a, kind: lax.all_gather(a.astype(kind), axis),
        array,
        jax.tree.map(lambda a: jnp.bfloat16 if a.dtype == jnp.float32 else a.dtype, array),
    )
    state = jax.tree.map(lambda a, e: jnp.zeros_like(a) + jnp.asarray(e, a.dtype), array, neutral)

    def one(hop, state):
        source = count - 1 - hop if backward else hop
        return join(
            state,
            jax.tree.map(
                lambda a, own: lax.dynamic_index_in_dim(a, source, 0, False).astype(own.dtype),
                gathered,
                array,
            ),
        )

    return lax.fori_loop(0, ahead, one, state)


def rotate(vectors, token_positions):
    half_width = vectors.shape[-1] // 2
    frequencies = ROPE_BASE ** (-jnp.arange(half_width, dtype=jnp.float32) / half_width)
    angles = token_positions.astype(jnp.float32)[:, None] * frequencies[None, :]
    cosine = jnp.cos(angles)[:, None, :]
    sine_part = jnp.sin(angles)[:, None, :]
    first_half = vectors[..., :half_width].astype(jnp.float32)
    second = vectors[..., half_width:].astype(jnp.float32)
    return jnp.concatenate(
        [first_half * cosine - second * sine_part, first_half * sine_part + second * cosine],
        axis=-1,
    )


def prepare(query_w, key_w, value_w, number_of_heads, token_positions):
    length = query_w.shape[0]
    queries_f = rotate(query_w.reshape(length, number_of_heads, -1), token_positions)
    key_dim = queries_f.shape[-1]
    queries = queries_f.astype(jnp.bfloat16)
    keys_rot = (
        rotate(key_w.reshape(length, number_of_heads, -1), token_positions)
        * (1.0 / math.sqrt(key_dim))
    ).astype(jnp.bfloat16)
    values = value_w.reshape(length, number_of_heads, -1)
    return (queries, keys_rot, values)


def sweep_blocks(queries, keys_rot, values, log_decay, strict, state_init, span_size):
    length, number_of_heads, key_dim = queries.shape
    value_dim = values.shape[-1]
    block_count = length // span_size

    def split_blocks(array):
        return array.reshape(block_count, span_size, number_of_heads, array.shape[-1])

    decay_blocks = log_decay.reshape(number_of_heads, block_count, span_size).transpose(1, 0, 2)
    position_index = jnp.arange(span_size)
    if strict:
        allowed = position_index[:, None] > position_index[None, :]
    else:
        allowed = position_index[:, None] >= position_index[None, :]

    def advance(state_now, inputs):
        query_blk, key_blk, value_blk, decay_blk = inputs
        cumulative = jnp.cumsum(decay_blk, axis=1)
        log_gap = cumulative[:, :, None] - cumulative[:, None, :]
        weights = jnp.where(allowed[None], jnp.exp(jnp.where(allowed[None], log_gap, 0.0)), 0.0)
        scores = (
            jnp.einsum("ihd,jhd->hij", query_blk, key_blk, preferred_element_type=jnp.float32)
            * weights
        )
        weighted = scores.astype(jnp.bfloat16)
        inner_part = jnp.einsum(
            "hij,jhv->ihv", weighted, value_blk, preferred_element_type=jnp.float32
        )
        carried = (
            jnp.einsum("ihd,hdv->ihv", query_blk.astype(jnp.float32), state_now, precision=HIGHEST)
            * jnp.exp(cumulative).T[:, :, None]
        )
        key_scaled = (
            key_blk.astype(jnp.float32) * jnp.exp(cumulative[:, -1:] - cumulative).T[:, :, None]
        )
        state_next = state_now * jnp.exp(cumulative[:, -1])[:, None, None] + jnp.einsum(
            "jhd,jhv->hdv", key_scaled, value_blk.astype(jnp.float32), precision=HIGHEST
        )
        return (state_next, inner_part + carried)

    final_state, outputs = lax.scan(
        advance,
        state_init,
        (split_blocks(queries), split_blocks(keys_rot), split_blocks(values), decay_blocks),
    )
    return (outputs.reshape(length, number_of_heads, value_dim), final_state)


def summary(keys_rot, values, log_decay):
    cumulative = jnp.cumsum(log_decay, axis=1)
    key_scaled = (
        keys_rot.astype(jnp.float32) * jnp.exp(cumulative[:, -1:] - cumulative).T[:, :, None]
    )
    return (
        jnp.exp(cumulative[:, -1]),
        jnp.einsum("lhd,lhv->hdv", key_scaled, values.astype(jnp.float32), precision=HIGHEST),
    )


def chain_states(earlier, later):
    decay_a0, state_a0, decay_b0, state_b0 = earlier
    decay_a1, state_a1, decay_b1, state_b1 = later
    return (
        decay_a0 * decay_a1,
        state_a0 * decay_a1[:, None, None] + state_a1,
        decay_b0 * decay_b1,
        state_b0 * decay_b1[:, None, None] + state_b1,
    )


def neutral(parts):
    return (
        jnp.ones_like(parts[0]),
        jnp.zeros_like(parts[1]),
        jnp.ones_like(parts[2]),
        jnp.zeros_like(parts[3]),
    )


def carry_states(forward_parts, backward_parts):
    into_forward = entering(forward_parts, "sp", chain_states, neutral(forward_parts), False)
    into_backward = entering(backward_parts, "sp", chain_states, neutral(backward_parts), True)
    return (into_forward, into_backward)


def finish(forward, backward_flipped):
    total_sum = forward + backward_flipped[::-1]
    normed = total_sum * lax.rsqrt(
        jnp.mean(total_sum * total_sum, axis=-1, keepdims=True) + GROUP_EPS
    )
    return normed.reshape(total_sum.shape[0], -1).astype(jnp.bfloat16)


def layer_norm(stream, gain):
    center = stream - jnp.mean(stream, axis=-1, keepdims=True)
    spread = jnp.mean(center * center, axis=-1, keepdims=True)
    return center * lax.rsqrt(spread + NORM_EPS) * gain


def slot_table(expert_ids):
    onehot = (expert_ids[..., None] == jnp.arange(EXPERTS, dtype=jnp.int32)).astype(jnp.int32)
    earlier = jnp.cumsum(onehot, axis=-2) - onehot
    rank_order = jnp.sum(earlier * onehot, axis=-1)
    kept_mask = rank_order < CAP
    slot_index = expert_ids * CAP + jnp.minimum(rank_order, CAP - 1)
    return (slot_index, kept_mask)


def gate_up(rows, gate_w, up_w):
    gate_part = jnp.einsum("xecd,edf->xecf", rows, gate_w, preferred_element_type=jnp.float32)
    up_part = jnp.einsum("xecd,edf->xecf", rows, up_w, preferred_element_type=jnp.float32)
    return (jax.nn.silu(gate_part) * up_part).astype(jnp.bfloat16)


def shards(
    query_a,
    key_a,
    value_a,
    decay_a,
    query_b,
    key_b,
    value_b,
    decay_b,
    out_weight_a,
    out_weight_b,
    residual,
    norm_gain,
    route_group,
    route_expert,
    route_weight,
    expert_gate,
    expert_up,
    expert_down,
):
    length = query_a.shape[0]
    token_positions = lax.axis_index("sp") * length + jnp.arange(length, dtype=jnp.int32)
    heads_a = decay_a.shape[1]
    heads_b = decay_b.shape[1]
    qa_rot, ka_rot, va_all = prepare(query_a, key_a, value_a, heads_a, token_positions)
    qb_rot, kb_rot, vb_all = prepare(query_b, key_b, value_b, heads_b, token_positions)
    flip_a = (qa_rot[::-1], ka_rot[::-1], va_all[::-1], decay_a[1][:, ::-1])
    flip_b = (qb_rot[::-1], kb_rot[::-1], vb_all[::-1], decay_b[1][:, ::-1])
    forward_parts = summary(ka_rot, va_all, decay_a[0]) + summary(kb_rot, vb_all, decay_b[0])
    backward_parts = summary(flip_a[1], flip_a[2], flip_a[3]) + summary(
        flip_b[1], flip_b[2], flip_b[3]
    )
    into_forward, into_backward = carry_states(forward_parts, backward_parts)
    forward_a = sweep_blocks(qa_rot, ka_rot, va_all, decay_a[0], False, into_forward[1], BLOCK)[0]
    forward_b = sweep_blocks(qb_rot, kb_rot, vb_all, decay_b[0], False, into_forward[3], BLOCK)[0]
    backward_a = sweep_blocks(
        flip_a[0], flip_a[1], flip_a[2], flip_a[3], True, into_backward[1], BLOCK
    )[0]
    backward_b = sweep_blocks(
        flip_b[0], flip_b[1], flip_b[2], flip_b[3], True, into_backward[3], BLOCK
    )[0]
    mixed_a = finish(forward_a, backward_a)
    mixed_b = finish(forward_b, backward_b)
    rows_dev = length // lax.axis_size("tp")
    mix = lax.psum_scatter(
        (
            jnp.dot(mixed_a, out_weight_a, preferred_element_type=jnp.float32)
            + jnp.dot(mixed_b, out_weight_b, preferred_element_type=jnp.float32)
        ).astype(jnp.bfloat16),
        "tp",
        scatter_dimension=0,
        tiled=True,
    ).astype(jnp.float32)
    hidden_in = layer_norm(
        RESIDUAL_SCALE * residual.astype(jnp.float32) + mix, norm_gain[0]
    ).astype(jnp.bfloat16)
    width = hidden_in.shape[1]
    ffn_width = expert_gate.shape[2]
    sp_count = lax.axis_size("sp")
    per_device = EXPERTS // sp_count
    slots = EXPERTS * CAP
    global_ids = (route_group[:, None] * EXP_GROUP + route_expert).reshape(-1)
    slot_index, kept_mask = slot_table(global_ids)
    hits = (slot_index[:, None] == jnp.arange(slots, dtype=jnp.int32)[None, :]) & kept_mask[:, None]
    choose = jnp.sum(hits.reshape(rows_dev, TOP, slots).astype(jnp.int32), axis=1).astype(
        jnp.bfloat16
    )
    outgoing = jnp.einsum(
        "rs,rd->sd", choose, hidden_in, preferred_element_type=jnp.float32
    ).astype(jnp.bfloat16)
    outgoing = outgoing.reshape(sp_count, per_device * CAP, width)
    received = lax.all_to_all(outgoing, "sp", split_axis=0, concat_axis=0, tiled=True)
    piece_rows = lax.all_gather(received, "tp", axis=0, tiled=True)
    piece_count = piece_rows.shape[0]
    shaped = piece_rows.reshape(-1, per_device, CAP, width)
    hidden = gate_up(shaped, expert_gate, expert_up).reshape(
        piece_count, per_device * CAP, ffn_width
    )
    flat_hidden = hidden.reshape(-1, ffn_width)
    piece_rows = flat_hidden.reshape(-1, per_device, CAP, ffn_width)
    summed = lax.psum_scatter(
        jnp.einsum("xecf,efd->xecd", piece_rows, expert_down, preferred_element_type=jnp.float32)
        .reshape(lax.axis_size("tp") * (sp_count * per_device * CAP), width)
        .astype(jnp.bfloat16),
        "tp",
        scatter_dimension=0,
        tiled=True,
    )
    back_rows = summed.reshape(sp_count, per_device * CAP, width)
    returned = lax.all_to_all(back_rows, "sp", split_axis=0, concat_axis=0, tiled=True).reshape(
        slots, width
    )
    picked = (
        jnp.take(returned, slot_index, axis=0).astype(jnp.float32).reshape(rows_dev, TOP, width)
    )
    factor = jnp.where(kept_mask.reshape(rows_dev, TOP), route_weight, 0.0)
    ffn = jnp.sum(picked * factor[..., None], axis=1)
    return layer_norm(RESIDUAL_SCALE * hidden_in.astype(jnp.float32) + ffn, norm_gain[1]).astype(
        jnp.bfloat16
    )


def solution(mesh):
    return jax.shard_map(
        shards,
        mesh=mesh,
        in_specs=(
            P(("grp", "sp"), "tp"),
            P(("grp", "sp"), "tp"),
            P(("grp", "sp"), "tp"),
            P(None, "tp", ("grp", "sp")),
            P(("grp", "sp"), "tp"),
            P(("grp", "sp"), "tp"),
            P(("grp", "sp"), "tp"),
            P(None, "tp", ("grp", "sp")),
            P("tp", None),
            P("tp", None),
            P(("grp", "sp", "tp"), None),
            P(),
            P(("grp", "sp", "tp")),
            P(("grp", "sp", "tp"), None),
            P(("grp", "sp", "tp"), None),
            P("sp", None, "tp"),
            P("sp", None, "tp"),
            P("sp", "tp", None),
        ),
        out_specs=P(("grp", "sp", "tp"), None),
        check_vma=False,
    )
```

profile of v0, /device:TPU:0, one launch (start us, length us, event | category | flops | bytes accessed | tf_op | source)
XLA Modules:
  0.0 341.4 jit_solution(14868243068585740529)
XLA Ops:
  13.9 1.7 rev.32
  28.9 1.8 reshape.586
  32.2 1.7 copy.291
  41.0 18.3 %all-gather.7 = bf16[16,64,64]{2,1,0:T(8,128)(2,1)S(1)} all-gather(bf16[4,64,64]{2,1,0:T(8,128)(2,1)S(1)} %convolution_convert_fusion.3), channel_id=9, replica_groups=mesh['grp'=2,'sp'=4,'tp'=4] {'sp'}, dimensions={0}, use_global_device_ids=true | all-gather | bytes 163840 | tf_op jit(solution)/shard_map/all_gather | solution.py:27
  65.7 11.8 %all-reduce.4 = (bf16[8]{0:T(256)(128)(2,1)S(1)}, bf16[16]{0:T(256)(128)(2,1)S(1)}, bf16[8]{0:T(256)(128)(2,1)S(1)}, bf16[16]{0:T(256)(128)(2,1)S(1)}) all-reduce(bf16[8]{0:T(256)(128)(2,1)S(1)} %dynamic-update-slice.2, bf16[16]{0:T(256)(128)(2,1)S(1)} %dynamic-update-slice.3, ...), channel_id=6, replica_groups=mesh['grp'=2,'sp'=4,'tp'=4] {'sp'}, use_global_device_ids=true, to_apply=%add.2 | all-reduce | flops 48 | bytes 192
  82.5 16.8 %all-gather.3 = bf16[16,64,64]{2,1,0:T(8,128)(2,1)} all-gather(bf16[4,64,64]{2,1,0:T(8,128)(2,1)S(1)} %convolution_convert_fusion.4), channel_id=5, replica_groups=mesh['grp'=2,'sp'=4,'tp'=4] {'sp'}, dimensions={0}, use_global_device_ids=true | all-gather | bytes 163840 | tf_op jit(solution)/shard_map/all_gather | solution.py:27
  106.0 1.7 pad_maximum_fusion
  107.9 6.6 %while.89 = (s32[]{:T(128)}, f32[2,256,512]{2,1,0:T(8,128)S(1)}, f32[4,64,64]{2,1,0:T(8,128)S(1)}, s32[]{:T(128)}, bf16[4,2]{1,0:T(4,128)(2,1)S(1)}, /*index=5*/...) while((s32[]{:T(128)}, f32[2,256,512]{2,1,0:T(8,128)S(1)}, ...), condition=%wide.region_14.15_spmd, body=%wide.region_13.14_spmd.sunk | while | flops 835596 | bytes 2785519 | solution.py:44
  114.5 8.4 %while.93 = (s32[]{:T(128)}, f32[4,64,64]{2,1,0:T(8,128)S(1)}, f32[2,128,4,64]{1,0,3,2:T(2,128)S(1)}, f32[2,4,128]{2,1,0:T(4,128)S(1)}, bf16[2,128,4,64]{1,3,2,0...) while((s32[]{:T(128)}, f32[4,64,64]{2,1,0:T(8,128)S(1)}, ...), condition=%wide.region_24.25_spmd.clone.clone, body=%wide.region_22.24_spmd.clone.clone.sunk | while | flops 67682304 | bytes 1434821 | solution.py:114
  115.8 2.6 dynamic_update_slice.31
  120.0 2.6 dynamic_update_slice.31
  125.2 20.7 %while.92 = (s32[]{:T(128)}, f32[4,64,64]{2,1,0:T(8,128)S(1)}, f32[2,128,4,64]{1,0,3,2:T(2,128)}, f32[2,4,128]{2,1,0:T(4,128)S(1)}, bf16[2,128,4,64]{1,3,2,0:T(8...) while((s32[]{:T(128)}, f32[4,64,64]{2,1,0:T(8,128)S(1)}, ...), condition=%wide.region_21.22_spmd.clone.clone, body=%wide.region_19.21_spmd.clone.clone.sunk | while | flops 67682304 | bytes 1303761 | solution.py:114
  125.8 1.8 fusion.315
  128.2 2.1 fusion.316
  130.2 4.2 %dynamic_update_slice.30 = f32[2,128,4,64]{1,0,3,2:T(2,128)} dynamic-update-slice(f32[2,128,4,64]{1,0,3,2:T(2,128)} %get-tuple-element.1233, f32[1,128,4,64]{1,0,3,2:T(1,128)} %bitcast.506, s32[]{:T(128)} %get-tuple-element.1231, s32[]{:T(128)} %constant.190.clone.1..sunk.2, s32[]{:T(128)} %constant.190.clone.1..sunk.2, s32[]{:T(128)} %constant.190.clone.1..sunk.2) | dynamic-update-slice | bytes 262148 | tf_op jit(solution)/shard_map/while/body/jit(dynamic_update_index_in_dim)/dynamic_update_slice | solution.py:114
  136.1 1.8 fusion.315
  138.5 2.1 fusion.316
  140.6 4.2 %dynamic_update_slice.30 = f32[2,128,4,64]{1,0,3,2:T(2,128)} dynamic-update-slice(f32[2,128,4,64]{1,0,3,2:T(2,128)} %get-tuple-element.1233, f32[1,128,4,64]{1,0,3,2:T(1,128)} %bitcast.506, s32[]{:T(128)} %get-tuple-element.1231, s32[]{:T(128)} %constant.190.clone.1..sunk.2, s32[]{:T(128)} %constant.190.clone.1..sunk.2, s32[]{:T(128)} %constant.190.clone.1..sunk.2) | dynamic-update-slice | bytes 262148 | tf_op jit(solution)/shard_map/while/body/jit(dynamic_update_index_in_dim)/dynamic_update_slice | solution.py:114
  145.9 1.9 reshape.525
  147.8 1.8 multiply_reduce_fusion.4
  150.7 24.6 %while.91 = (s32[]{:T(128)}, f32[2,256,512]{2,1,0:T(8,128)S(1)}, f32[2,128,2,512]{3,1,0,2:T(8,128)}, f32[2,2,128]{2,1,0:T(2,128)}, bf16[2,128,2,256]{3,1,0,2:T(8...) while((s32[]{:T(128)}, f32[2,256,512]{2,1,0:T(8,128)S(1)}, ...), condition=%wide.region_17.18_spmd.clone.clone, body=%wide.region_15.17_spmd.clone.clone.sunk | while | flops 856768512 | bytes 7912589 | solution.py:114
  151.7 2.2 convolution_bitcast_fusion.9
  154.2 3.0 fusion.307
  157.1 2.0 copy.414
  159.2 1.9 constant_dynamic-update-slice_fusion.5
  161.0 2.0 convolution_add_fusion.10
  164.0 2.2 convolution_bitcast_fusion.9
  166.5 3.0 fusion.307
  169.4 2.0 copy.414
  171.5 1.9 constant_dynamic-update-slice_fusion.5
  173.4 2.0 convolution_add_fusion.10
  175.4 8.9 %rev.37 = f32[256,2,512]{2,0,1:T(8,128)} reverse(f32[256,2,512]{2,0,1:T(8,128)} %bitcast.502), dimensions={0} | reverse | bytes 2097152 | tf_op jit(solution)/shard_map/rev | solution.py:160
  185.4 18.0 %while.90 = (s32[]{:T(128)}, f32[2,256,512]{2,1,0:T(8,128)S(1)}, f32[2,128,2,512]{3,1,0,2:T(8,128)}, f32[2,2,128]{2,1,0:T(2,128)S(1)}, bf16[2,128,2,256]{3,1,0,2...) while((s32[]{:T(128)}, f32[2,256,512]{2,1,0:T(8,128)S(1)}, ...), condition=%wide.region_8.9_spmd.clone.clone, body=%wide.region_6.8_spmd.clone.clone.sunk | while | flops 856768512 | bytes 9483953 | solution.py:114
  188.5 2.8 fusion.298
  197.6 2.8 fusion.298
  203.5 1.8 multiply_reduce_fusion.1
  205.2 1.7 multiply_convert_fusion
  207.2 3.5 %fusion.231 = f32[256,2048]{1,0:T(8,128)S(1)} fusion(bf16[256,1024]{0,1:T(8,128)(2,1)S(1)} %bitcast.517, bf16[1024,2048]{1,0:T(8,128)(2,1)} %param.38), kind=kOutput, calls=%fused_computation.337 | convolution fusion | flops 1073741824 | bytes 6815744 | tf_op jit(solution)/shard_map/dot_general | solution.py:234
  213.6 27.6 %reduce-scatter.3.cloned.1.call-done = bf16[64,2048]{1,0:T(8,128)(2,1)} async-done(((bf16[256,2048]{1,0:T(8,128)(2,1)}), bf16[64,2048]{1,0:T(8,128)(2,1)}) %reduce-scatter.3.cloned.1.call-update) | async-done | bytes 262160 | tf_op jit(solution)/shard_map/reduce_scatter | solution.py:232
  245.0 13.2 %all_to_all.10 = bf16[4,16,2048]{2,1,0:T(8,128)(2,1)} all-to-all(bf16[4,16,2048]{2,1,0:T(8,128)(2,1)S(1)} %bitcast.513), channel_id=1, replica_groups=mesh['grp'=2,'sp'=4,'tp'=4] {'sp'}, dimensions={0} | all-to-all | bytes 524288 | tf_op jit(solution)/shard_map/all_to_all | solution.py:259
  258.4 14.7 %all-gather.12.cloned.1.call-done = bf16[16,16,2048]{2,1,0:T(8,128)(2,1)} async-done(((bf16[4,16,2048]{2,1,0:T(8,128)(2,1)}), bf16[16,16,2048]{2,1,0:T(8,128)(2,1)}) %all-gather.12.cloned.1.call-update) | async-done | bytes 1048592 | tf_op jit(solution)/shard_map/all_gather | solution.py:260
  273.2 1.8 copy.326
  275.0 5.6 %fusion.173 = f32[16,8,2,256]{3,0,2,1:T(8,128)} fusion(bf16[16,8,2,2048]{3,0,2,1:T(8,128)(2,1)S(1)} %bitcast.496, bf16[8,2048,256]{2,1,0:T(8,128)(2,1)} %param.45), kind=kOutput, calls=%fused_computation.196 | convolution fusion | flops 268435456 | bytes 9699328 | tf_op jit(solution)/shard_map/xecd,edf->xecf/dot_general | solution.py:183
  280.6 8.7 %fusion.170 = bf16[16,8,2,2048]{3,0,2,1:T(8,128)(2,1)S(1)} fusion(bf16[8,256,2048]{2,1,0:T(8,128)(2,1)} %param.47, bf16[16,8,2,2048]{3,0,2,1:T(8,128)(2,1)S(1)} %bitcast.497, bf16[8,2048,256]{2,1,0:T(8,128)(2,1)} %param.46, f32[16,8,2,256]{3,0,2,1:T(8,128)} %fusion.173), kind=kOutput, calls=%fused_computation.192 | convolution fusion | flops 537788416 | bytes 19136512 | tf_op jit(solution)/shard_map/xecf,efd->xecd/dot_general | solution.py:269
  291.9 24.7 %reduce-scatter.5.cloned.1.call-done = bf16[64,2048]{1,0:T(8,128)(2,1)} async-done(((bf16[256,2048]{1,0:T(8,128)(2,1)}), bf16[64,2048]{1,0:T(8,128)(2,1)}) %reduce-scatter.5.cloned.1.call-update) | async-done | bytes 262160 | tf_op jit(solution)/shard_map/reduce_scatter | solution.py:268
  316.6 4.6 %all-to-all-start.1 = ((bf16[4,16,2048]{2,1,0:T(8,128)(2,1)}), bf16[4,16,2048]{2,1,0:T(8,128)(2,1)S(1)}, u32[]{:S(2)}, u32[]{:S(2)}) async-start(bf16[4,16,2048]{2,1,0:T(8,128)(2,1)} %bitcast.522), calls=%async_computation.3 | async-start | bytes 524288 | tf_op jit(solution)/shard_map/all_to_all | solution.py:277
  321.4 8.5 %all-to-all-done.1 = bf16[4,16,2048]{2,1,0:T(8,128)(2,1)S(1)} async-done(((bf16[4,16,2048]{2,1,0:T(8,128)(2,1)}), bf16[4,16,2048]{2,1,0:T(8,128)(2,1)S(1)}, u32[]{:S(2)}, u32[]{:S(2)}) %all-to-all-start.1) | async-done | bytes 262176 | tf_op jit(solution)/shard_map/all_to_all | solution.py:277
  331.2 2.3 multiply_reduce_fusion
  (298 shorter events, 92.0 us)
Async XLA Ops:
  6.5 204.2 %copy-start = (bf16[256,2048]{1,0:T(8,128)(2,1)S(1)}, bf16[256,2048]{1,0:T(8,128)(2,1)}, u32[]{:S(2)}) copy-start(bf16[256,2048]{1,0:T(8,128)(2,1)} %param.39) | copy-start | bytes 3145732
  6.5 4.6 %copy-start.15 = (f32[2,2,256]{2,1,0:T(2,128)S(1)}, f32[2,2,256]{2,1,0:T(2,128)}, u32[]{:S(2)}) copy-start(f32[2,2,256]{2,1,0:T(2,128)} %param.33) | copy-start | bytes 12292
  6.5 7.2 %copy-start.3 = (bf16[256,1024]{1,0:T(8,128)(2,1)S(1)}, bf16[256,1024]{1,0:T(8,128)(2,1)}, u32[]{:S(2)}) copy-start(bf16[256,1024]{1,0:T(8,128)(2,1)} %param.32) | copy-start | bytes 1572868
  6.5 101.2 %all-gather.16.cloned.1.call-start = ((), (), s32[]{:S(2)}) async-start(), calls=%async_computation.8 | async-start | bytes 2621440 | tf_op jit(solution)/shard_map/all_gather | solution.py:27
  9.4 13.2 %copy-start.10 = (bf16[256,256]{1,0:T(8,128)(2,1)S(1)}, bf16[256,256]{1,0:T(8,128)(2,1)}, u32[]{:S(2)}) copy-start(bf16[256,256]{1,0:T(8,128)(2,1)} %param.35) | copy-start | bytes 393220
  9.4 13.3 %copy-start.11 = (bf16[256,256]{1,0:T(8,128)(2,1)S(1)}, bf16[256,256]{1,0:T(8,128)(2,1)}, u32[]{:S(2)}) copy-start(bf16[256,256]{1,0:T(8,128)(2,1)} %param.34) | copy-start | bytes 393220
  11.9 1.2 copy-start.12
  13.1 0.5 copy-start.18
  17.0 107.0 %all-gather.14.cloned.1.call-start = ((), (), s32[]{:S(2)}) async-start(), calls=%async_computation.7 | async-start | bytes 2621440 | tf_op jit(solution)/shard_map/all_gather | solution.py:27
  19.8 16.4 %copy-start.4 = (bf16[256,1024]{1,0:T(8,128)(2,1)S(1)}, bf16[256,1024]{1,0:T(8,128)(2,1)}, u32[]{:S(2)}) copy-start(bf16[256,1024]{1,0:T(8,128)(2,1)} %param.32) | copy-start | bytes 1572868
  19.9 221.4 %reduce-scatter.3.cloned.1.call-start = ((), (), s32[]{:S(2)}) async-start(), calls=%async_computation.4 | async-start | bytes 1310720 | tf_op jit(solution)/shard_map/reduce_scatter | solution.py:232
  28.9 11.9 %copy-start.5 = (bf16[256,256]{0,1:T(8,128)(2,1)}, bf16[256,256]{0,1:T(8,128)(2,1)S(1)}, u32[]{:S(2)}) copy-start(bf16[256,256]{0,1:T(8,128)(2,1)S(1)} %copy.287) | copy-start | bytes 393220
  32.0 70.8 %copy-start.7 = (bf16[2,128,4,64]{3,2,1,0:T(4,128)(2,1)S(1)}, bf16[2,128,4,64]{3,2,1,0:T(4,128)(2,1)}, u32[]{:S(2)}) copy-start(bf16[2,128,4,64]{3,2,1,0:T(4,128)(2,1)} %reshape.586) | copy-start | bytes 393220
  36.2 63.2 %copy-start.9 = (f32[2,128,4,32]{1,0,3,2:T(2,128)S(1)}, f32[2,128,4,32]{1,0,3,2:T(2,128)}, u32[]{:S(2)}) copy-start(f32[2,128,4,32]{1,0,3,2:T(2,128)} %concatenate.53) | copy-start | bytes 393220
  37.4 66.2 %copy-start.8 = (bf16[256,2,256]{0,2,1:T(8,128)(2,1)S(1)}, bf16[256,2,256]{0,2,1:T(8,128)(2,1)}, u32[]{:S(2)}) copy-start(bf16[256,2,256]{0,2,1:T(8,128)(2,1)} %pad_maximum_fusion.1) | copy-start | bytes 786436
  82.5 25.4 %copy-start.21 = (bf16[4,2]{1,0:T(4,128)(2,1)S(1)}, bf16[4,2]{1,0:T(4,128)(2,1)}, u32[]{:S(2)}) copy-start(bf16[4,2]{1,0:T(4,128)(2,1)} %reshape.555) | copy-start | bytes 52
  114.5 9.7 %copy-start.20 = (bf16[4,2]{1,0:T(4,128)(2,1)S(1)}, bf16[4,2]{1,0:T(4,128)(2,1)}, u32[]{:S(2)}) copy-start(bf16[4,2]{1,0:T(4,128)(2,1)} %reshape.551) | copy-start | bytes 52
  150.7 34.7 %copy-start.13 = (f32[2,2,128]{2,1,0:T(2,128)S(1)}, f32[2,2,128]{2,1,0:T(2,128)}, u32[]{:S(2)}) copy-start(f32[2,2,128]{2,1,0:T(2,128)} %get-tuple-element.1197) | copy-start | bytes 6148
  185.4 8.0 %copy-start.1 = (bf16[2,128,2,256]{3,1,0,2:T(8,128)(2,1)S(1)}, bf16[2,128,2,256]{3,1,0,2:T(8,128)(2,1)}, u32[]{:S(2)}) copy-start(bf16[2,128,2,256]{3,1,0,2:T(8,128)(2,1)} %get-tuple-element.1216) | copy-start | bytes 786436 | tf_op jit(solution)/shard_map/while
  194.4 8.0 %copy-start.1 = (bf16[2,128,2,256]{3,1,0,2:T(8,128)(2,1)S(1)}, bf16[2,128,2,256]{3,1,0,2:T(8,128)(2,1)}, u32[]{:S(2)}) copy-start(bf16[2,128,2,256]{3,1,0,2:T(8,128)(2,1)} %get-tuple-element.1216) | copy-start | bytes 786436 | tf_op jit(solution)/shard_map/while
  203.5 3.7 %copy-start.6 = (f32[256,4,64]{0,2,1:T(8,128)S(1)}, f32[256,4,64]{0,2,1:T(8,128)}, u32[]{:S(2)}) copy-start(f32[256,4,64]{0,2,1:T(8,128)} %get-tuple-element.775) | copy-start | bytes 786436
  210.6 1.6 copy-start.19
  210.7 1.6 copy-start.16
  210.7 2.9 copy-start.14
  210.7 30.6 %copy-start.2 = (bf16[64,2048]{1,0:T(8,128)(2,1)S(1)}, bf16[64,2048]{1,0:T(8,128)(2,1)}, u32[]{:S(2)}) copy-start(bf16[64,2048]{1,0:T(8,128)(2,1)} %param.40) | copy-start | bytes 786436
  212.2 61.0 %all-gather.12.cloned.1.call-start = ((), (), s32[]{:S(2)}) async-start(), calls=%async_computation.5 | async-start | bytes 1310720 | tf_op jit(solution)/shard_map/all_gather | solution.py:260
  258.2 58.4 %reduce-scatter.5.cloned.1.call-start = ((), (), s32[]{:S(2)}) async-start(), calls=%async_computation.6 | async-start | bytes 1310720 | tf_op jit(solution)/shard_map/reduce_scatter | solution.py:268
  289.3 32.1 %copy-start.17 = (f32[64,2]{0,1:T(2,128)S(1)}, f32[64,2]{0,1:T(2,128)}, u32[]{:S(2)}) copy-start(f32[64,2]{0,1:T(2,128)} %param.44) | copy-start | bytes 1540
  316.6 13.3 %all-to-all-start.1 = ((bf16[4,16,2048]{2,1,0:T(8,128)(2,1)}), bf16[4,16,2048]{2,1,0:T(8,128)(2,1)S(1)}, u32[]{:S(2)}, u32[]{:S(2)}) async-start(bf16[4,16,2048]{2,1,0:T(8,128)(2,1)} %bitcast.522), calls=%async_computation.3 | async-start | bytes 524288 | tf_op jit(solution)/shard_map/all_to_all | solution.py:277
Sparse Core Ops, SparseCore 0:
  17.2 52.6 all-gather.15
  71.4 48.6 all-gather.13
  212.3 28.8 reduce-scatter.2
  258.3 14.8 all-gather.11
  291.8 24.8 reduce-scatter.4
where the time goes:
time: 344 us; the launch traced here: 341 us
  local copies, waits for them, and re-layouts  84.7 us (25%)
  waiting for transfers between devices  75.7 us (22%)
  blocking collectives  60.1 us (17%)
  matrix products  60 us (17%)
  other arithmetic  40.3 us (12%)
  between operations  15 us (4%)
  starting transfers between devices  4.99 us (1%)
    all_gather x2, blocking collectives, entering(): lax.all_gather(a.astype(kind), axis)  35.1 us
    reduce_scatter x1, waiting for transfers between devices, shards(): lax.psum_scatter((jnp.dot(mixed_a, out_weight_a, preferred_element_type=j...  27.6 us
    dynamic_update_slice x12, local copies, waits for them, and re-layouts, sweep_blocks(): lax.scan(advance, state_init, (split_blocks(queries), split_blocks(keys_r...  25.6 us
    reduce_scatter x1, waiting for transfers between devices, shards(): lax.psum_scatter(jnp.einsum('xecf,efd->xecd', piece_rows, expert_down, pr...  24.7 us
    dot_general x8, matrix products, advance(): jnp.einsum('ihd,hdv->ihv', query_blk.astype(jnp.float32), state_now, prec...  15.6 us
    all_gather x1, waiting for transfers between devices, shards(): piece_rows = lax.all_gather(received, 'tp', axis=0, tiled=True)  14.7 us
    all_to_all x1, blocking collectives, shards(): lax.all_to_all(outgoing, 'sp', split_axis=0, concat_axis=0, tiled=True)  13.2 us
    dot_general x8, matrix products, advance(): jnp.einsum('hij,jhv->ihv', weighted, value_blk, preferred_element_type=jn...  12 us
  transfers between devices with their start and end apart: 6, of which 4 were waited for; matrix products, arithmetic and copies ran while one was open for 18% of the time, Pallas kernels for 0%

commit v1 on v0

--- a/solution.py
+++ b/solution.py
@@ -1,8 +1,12 @@
+import functools
 import math
 
 import jax
 import jax.numpy as jnp
 from jax import lax
+import numpy as np
+from jax.experimental import pallas as pl
+from jax.experimental.pallas import tpu as pltpu
 from jax.sharding import PartitionSpec as P
 
 BLOCK = 128
@@ -287,9 +291,718 @@
     )
 
 
+MESH = pl.DeviceIdType.MESH
+F32 = jnp.float32
+BF16 = jnp.bfloat16
+NT = (((1,), (1,)), ((), ()))
+TN = (((0,), (0,)), ((), ()))
+LANES = 128
+
+
+def dot(a, b, dims=None, precision=None):
+    dims = dims or (((1,), (0,)), ((), ()))
+    return lax.dot_general(a, b, dims, precision=precision, preferred_element_type=F32)
+
+
+def layer_kernel(
+    cfg,
+    qa,
+    ka,
+    va,
+    qb,
+    kb,
+    vb,
+    dec,
+    cos_a,
+    sin_a,
+    cos_b,
+    sin_b,
+    head_mask,
+    block_mask,
+    rope_perm,
+    sort_rows,
+    unsort_rows,
+    woa,
+    wob,
+    res,
+    gain,
+    rg,
+    re,
+    rw,
+    eg,
+    eu,
+    ed,
+    out,
+    wo_v,
+    eg_v,
+    eu_v,
+    ed_v,
+    qa_s,
+    ka_s,
+    qb_s,
+    kb_s,
+    acc_a,
+    acc_b,
+    mixed,
+    loc,
+    loc_b,
+    dfs,
+    dfs_b,
+    cin,
+    cin_b,
+    cout,
+    cout_b,
+    p_out,
+    p_in,
+    x_out,
+    x_in,
+    own,
+    gbuf,
+    obuf,
+    xs,
+    ys,
+    ep_out,
+    ep_in,
+    ex_out,
+    ex_in,
+    ret,
+    fin,
+    w_sem,
+    wo_sem,
+    c_send,
+    c_recv,
+    cb_send,
+    cb_recv,
+    p_send,
+    p_recv,
+    x_send,
+    x_recv,
+    d_send,
+    g_send,
+    g_recv,
+    ep_send,
+    ep_recv,
+    ex_send,
+    ex_recv,
+    r_send,
+    r_recv,
+):
+    nsp, ntp, ha, hb = cfg["nsp"], cfg["ntp"], cfg["ha"], cfg["hb"]
+    half = ntp // 2
+    length, width = qa.shape[0], res.shape[1]
+    dka, dva = qa.shape[1] // ha, va.shape[1] // ha
+    dkb = qb.shape[1] // hb
+    rows = length // ntp
+    cph = dva // LANES
+    chunks = ha * cph
+    sp, tp = lax.axis_index("sp"), lax.axis_index("tp")
+    pair = tp // 2
+    core = tp % 2
+    mate = 2 * pair + 1 - core
+    per_dev = eg.shape[0]
+    tiles = p_out.shape[0]
+    tile = width // tiles
+
+    wo_copies = [
+        pltpu.make_async_copy(woa, wo_v.at[pl.ds(0, ha * dva)], wo_sem.at[0]),
+        pltpu.make_async_copy(wob, wo_v.at[pl.ds(ha * dva, wob.shape[0])], wo_sem.at[1]),
+    ]
+    for c in wo_copies:
+        c.start()
+
+    def weight_copies(e):
+        return [
+            pltpu.make_async_copy(a.at[e], b.at[e], w_sem.at[i, e])
+            for i, (a, b) in enumerate(((eg, eg_v), (eu, eu_v), (ed, ed_v)))
+        ]
+
+    @pl.loop(0, per_dev)
+    def _(e):
+        for c in weight_copies(e):
+            c.start()
+
+    barrier = pltpu.get_barrier_semaphore()
+    for d in range(1, nsp):
+        pl.semaphore_signal(
+            barrier, inc=1, device_id={"sp": (sp + d) % nsp}, device_id_type=MESH
+        )
+    for d in range(1, ntp):
+        pl.semaphore_signal(
+            barrier, inc=1, device_id={"tp": (tp + d) % ntp}, device_id_type=MESH
+        )
+
+    def remote(src, dst, ssem, rsem, axis, where):
+        return pltpu.make_async_remote_copy(
+            src_ref=src,
+            dst_ref=dst,
+            send_sem=ssem,
+            recv_sem=rsem,
+            device_id={axis: where},
+            device_id_type=MESH,
+        )
+
+    r_i = lax.broadcasted_iota(jnp.int32, (length, length), 0)
+    c_i = lax.broadcasted_iota(jnp.int32, (length, length), 1)
+    lower = r_i >= c_i
+    tri = jnp.where(lower, 1.0, 0.0).astype(F32)
+    tri_s = jnp.where(r_i > c_i, 1.0, 0.0).astype(F32)
+    d = dec[...]
+    inc_col = dot(tri, d, NT, HIGHEST)
+    inc_row = dot(d, tri, NT, HIGHEST)
+    exc_col = dot(tri_s, d, NT, HIGHEST)
+    exc_row = dot(d, tri_s, NT, HIGHEST)
+    total = inc_row[:, length - 1 : length]
+
+    def index(kind, back, h):
+        return (0 if kind == "a" else 2 * ha) + (hb if kind == "b" else ha) * back + h
+
+    def tot(kind, back, h):
+        i = index(kind, back, h)
+        return total[i : i + 1, :]
+
+    def col(arr, kind, back, h):
+        i = index(kind, back, h)
+        return arr[:, i : i + 1]
+
+    def row(arr, kind, back, h):
+        i = index(kind, back, h)
+        return arr[i : i + 1, :]
+
+    hw = dka // 2
+    ca, sa = cos_a[...], sin_a[...]
+
+    def rot_a(x, scale):
+        x1, x2 = x[:, :hw].astype(F32), x[:, hw:].astype(F32)
+        y = jnp.concatenate([x1 * ca - x2 * sa, x1 * sa + x2 * ca], axis=1)
+        return (y * scale).astype(BF16)
+
+    masks = [head_mask[j : j + 1, :] for j in range(hb)]
+    bm = block_mask[...]
+    vbv = vb[...]
+
+    def rot_b(x, scale):
+        y = x.astype(F32) * cos_b[...] + dot(x, rope_perm[...]) * sin_b[...]
+        return (y * scale).astype(BF16)
+
+    def spread(cols):
+        return functools.reduce(lambda x, y: x + y, [c * m for c, m in zip(cols, masks)])
+
+    kbr = rot_b(kb[...], 1.0 / math.sqrt(dkb))
+    kb_s[...] = kbr
+    for back in (0, 1):
+        if back:
+            scale = spread([jnp.exp(col(exc_col, "b", 1, j)) for j in range(hb)])
+        else:
+            scale = spread(
+                [jnp.exp(tot("b", 0, j) - col(inc_col, "b", 0, j)) for j in range(hb)]
+            )
+        full = dot((kbr.astype(F32) * scale).astype(BF16), vbv, TN) * bm
+        loc_b[back] = functools.reduce(
+            lambda x, y: x + y, [full[j * dkb : (j + 1) * dkb] for j in range(hb)]
+        )
+        dfs_b[back] = jnp.broadcast_to(
+            spread([jnp.exp(tot("b", back, j)) for j in range(hb)]), dfs_b.shape[1:]
+        )
+    for h in range(ha):
+        k = rot_a(ka[:, h * dka : (h + 1) * dka], 1.0 / math.sqrt(dka))
+        ka_s[:, h * dka : (h + 1) * dka] = k
+        kf = k.astype(F32)
+        for back in (0, 1):
+            if back:
+                scale = jnp.exp(col(exc_col, "a", 1, h))
+            else:
+                scale = jnp.exp(tot("a", 0, h) - col(inc_col, "a", 0, h))
+            state = dot((kf * scale).astype(BF16), va[:, h * dva : (h + 1) * dva], TN)
+            for c in range(cph):
+                loc[back, h * cph + c] = state[:, c * LANES : (c + 1) * LANES]
+                dfs[back, h * cph + c] = jnp.broadcast_to(
+                    jnp.exp(tot("a", back, h)), dfs.shape[2:]
+                )
+
+    pl.semaphore_wait(barrier, nsp - 1 + ntp - 1)
+
+    @pl.when(sp == 0)
+    def _():
+        cin[0] = jnp.zeros(cin.shape[1:], BF16)
+        cin_b[0] = jnp.zeros(cin_b.shape[1:], BF16)
+
+    @pl.when(sp == nsp - 1)
+    def _():
+        cin[1] = jnp.zeros(cin.shape[1:], BF16)
+        cin_b[1] = jnp.zeros(cin_b.shape[1:], BF16)
+
+    def chain_copy(back, c):
+        to = (sp + nsp - 1) % nsp if back else (sp + 1) % nsp
+        return remote(
+            cout.at[back, c], cin.at[back, c], c_send.at[back, c], c_recv.at[back, c], "sp", to
+        )
+
+    def chain_copy_b(back):
+        to = (sp + nsp - 1) % nsp if back else (sp + 1) % nsp
+        return remote(
+            cout_b.at[back], cin_b.at[back], cb_send.at[back], cb_recv.at[back], "sp", to
+        )
+
+    def chain(back, t):
+        place = nsp - 1 - sp if back else sp
+        c = t - place
+
+        @pl.when((c >= 0) & (c < chunks))
+        def _():
+            @pl.when(place > 0)
+            def _():
+                chain_copy(back, c).wait_recv()
+
+            @pl.when(place < nsp - 1)
+            def _():
+                cout[back, c] = (
+                    cin[back, c].astype(F32) * dfs[back, c][:1] + loc[back, c]
+                ).astype(BF16)
+                chain_copy(back, c).start()
+
+        @pl.when(c == 0)
+        def _():
+            @pl.when(place > 0)
+            def _():
+                chain_copy_b(back).wait_recv()
+
+            @pl.when(place < nsp - 1)
+            def _():
+                cout_b[back] = (
+                    cin_b[back].astype(F32) * dfs_b[back][:1] + loc_b[back]
+                ).astype(BF16)
+                chain_copy_b(back).start()
+
+    def weights(kind, h):
+        ahead = col(inc_col, kind, 0, h) - row(inc_row, kind, 0, h)
+        behind = row(exc_row, kind, 1, h) - col(exc_col, kind, 1, h)
+        return jnp.exp(jnp.minimum(jnp.where(lower, ahead, behind), 0.0))
+
+    def local_a(h):
+        q = rot_a(qa[:, h * dka : (h + 1) * dka], 1.0)
+        qa_s[:, h * dka : (h + 1) * dka] = q
+        s = dot(q, ka_s[:, h * dka : (h + 1) * dka], NT) * weights("a", h)
+        acc_a[:, h * dva : (h + 1) * dva] = dot(
+            s.astype(BF16), va[:, h * dva : (h + 1) * dva]
+        )
+
+    def local_b(j):
+        if j == 0:
+            qb_s[...] = rot_b(qb[...], 1.0)
+        q = (qb_s[...].astype(F32) * masks[j]).astype(BF16)
+        s = dot(q, kb_s[...], NT) * weights("b", j)
+        part = dot(s.astype(BF16), vb[...]) * masks[j]
+        if j:
+            acc_b[...] += part
+        else:
+            acc_b[...] = part
+
+    work = [functools.partial(local_a, h) for h in range(ha)]
+    work += [functools.partial(local_b, j) for j in range(hb)]
+    steps = chunks + nsp - 1
+    for t in range(steps):
+        chain(0, t)
+        chain(1, t)
+        if t < len(work):
+            work[t]()
+    for piece in work[steps:]:
+        piece()
+
+    for h in range(ha):
+        q = qa_s[:, h * dka : (h + 1) * dka]
+        parts = []
+        for back in (0, 1):
+            state = jnp.concatenate([cin[back, h * cph + c] for c in range(cph)], axis=1)
+            if back:
+                scale = jnp.exp(tot("a", 1, h) - col(exc_col, "a", 1, h))
+            else:
+                scale = jnp.exp(col(inc_col, "a", 0, h))
+            parts.append(dot(q, state) * scale)
+        y = acc_a[:, h * dva : (h + 1) * dva] + parts[0] + parts[1]
+        y = y * lax.rsqrt(jnp.mean(y * y, axis=-1, keepdims=True) + GROUP_EPS)
+        mixed[:, h * dva : (h + 1) * dva] = y.astype(BF16)
+    y = acc_b[...]
+    for back in (0, 1):
+        state = jnp.concatenate([cin_b[back].astype(F32)] * hb, axis=0) * bm
+        if back:
+            scale = spread([jnp.exp(tot("b", 1, j) - col(exc_col, "b", 1, j)) for j in range(hb)])
+        else:
+            scale = spread([jnp.exp(col(inc_col, "b", 0, j)) for j in range(hb)])
+        y = y + dot(qb_s[...], state.astype(BF16)) * scale
+    square = dot(y * y, bm, None, HIGHEST) * (1.0 / dkb)
+    mixed[:, ha * dva :] = (y * lax.rsqrt(square + GROUP_EPS)).astype(BF16)
+
+    for c in wo_copies:
+        c.wait()
+
+    def block(i):
+        return mixed[pl.ds(pl.multiple_of(i * rows, rows), rows), :]
+
+    theirs = jnp.concatenate([block(2 * i + 1 - core) for i in range(half)], axis=0)
+    mine = jnp.concatenate([block(2 * i + core) for i in range(half)], axis=0)
+
+    def p_copy(n):
+        return remote(p_out.at[n], p_in.at[n], p_send.at[n], p_recv.at[n], "tp", mate)
+
+    def x_copy(n, k):
+        i = (pair + k) % half
+        return remote(
+            x_out.at[k - 1, n],
+            x_in.at[k - 1, n],
+            x_send.at[k - 1, n],
+            x_recv.at[k - 1, n],
+            "tp",
+            2 * i + core,
+        )
+
+    for n in range(tiles):
+        p_out[n] = dot(theirs, wo_v[:, n * tile : (n + 1) * tile]).astype(BF16)
+        p_copy(n).start()
+    for n in range(tiles):
+        own[n] = dot(mine, wo_v[:, n * tile : (n + 1) * tile])
+        p_copy(n).wait_recv()
+        own[n] += p_in[n].astype(F32)
+        for k in range(1, half):
+            i = (pair + k) % half
+            x_out[k - 1, n] = own[n, pl.ds(pl.multiple_of(i * rows, rows), rows), :].astype(BF16)
+            x_copy(n, k).start()
+    mix = []
+    for n in range(tiles):
+        m = own[n, pl.ds(pl.multiple_of(pair * rows, rows), rows), :]
+        for k in range(1, half):
+            x_copy(n, k).wait_recv()
+            m = m + x_in[k - 1, n].astype(F32)
+        mix.append(m)
+    mix = jnp.concatenate(mix, axis=1)
+
+    def norm(x, g):
+        x = x - jnp.mean(x, axis=-1, keepdims=True)
+        return x * lax.rsqrt(jnp.mean(x * x, axis=-1, keepdims=True) + NORM_EPS) * g
+
+    hidden = norm(RESIDUAL_SCALE * res[...].astype(F32) + mix, gain[0:1, :]).astype(BF16)
+
+    slots = EXPERTS * CAP
+    lane_e = lax.broadcasted_iota(jnp.int32, (rows, EXPERTS), 1)
+    lane_s = lax.broadcasted_iota(jnp.int32, (rows, slots), 1)
+    ids = [rg[...] * EXP_GROUP + re[:, k : k + 1] for k in range(TOP)]
+    hot = [jnp.where(i == lane_e, 1.0, 0.0) for i in ids]
+    before = jnp.where(
+        lax.broadcasted_iota(jnp.int32, (rows, rows), 0)
+        > lax.broadcasted_iota(jnp.int32, (rows, rows), 1),
+        1.0,
+        0.0,
+    )
+    earlier = dot(before.astype(BF16), functools.reduce(jnp.add, hot).astype(BF16))
+    choose = []
+    for i, o in zip(ids, hot):
+        rank = jnp.sum(earlier * o, axis=1, keepdims=True)
+        hit = jnp.zeros((rows, slots), F32)
+        for c in range(CAP):
+            hit = hit + jnp.where((lane_s == i * CAP + c) & (rank == float(c)), 1.0, 0.0)
+        choose.append(hit)
+    outgoing = dot(functools.reduce(jnp.add, choose).astype(BF16), hidden, TN).astype(BF16)
+    piece = per_dev * CAP
+    for s in range(nsp):
+        obuf[s] = outgoing[s * piece : (s + 1) * piece]
+
+    def d_copy(k):
+        to = (sp + k) % nsp
+        return remote(
+            obuf.at[to], gbuf.at[tp, sp], d_send.at[k - 1], g_recv.at[tp, sp], "sp", to
+        )
+
+    def g_copy(t, s, to, which, k):
+        return remote(
+            gbuf.at[t, s], gbuf.at[t, s], g_send.at[which, k], g_recv.at[t, s], "tp", to
+        )
+
+    def relay(s, k):
+        for j in range(1, half):
+            g_copy(tp, s, 2 * ((pair + j) % half) + core, j, k).start()
+        g_copy(tp, s, mate, 0, k).start()
+
+    order = sorted(range(1, nsp), key=lambda k: -min(k, nsp - k))
+    for k in order:
+        d_copy(k).start()
+    gbuf[tp, sp] = obuf[sp]
+    relay(sp, 0)
+    for k in range(1, nsp):
+        s = (sp + k) % nsp
+        g_copy(tp, s, mate, 0, k).wait_recv()
+        relay(s, k)
+    for k in range(nsp):
+        s = (sp + k) % nsp
+        for j in range(1, half):
+            t = 2 * ((pair + j) % half) + core
+            g_copy(t, s, mate, 0, k).wait_recv()
+            g_copy(t, s, mate, half + j - 1, k).start()
+    for i in range(half):
+        for k in range(nsp):
+            g_copy(2 * i + 1 - core, (sp + k) % nsp, mate, 0, k).wait_recv()
+
+    count = ntp * nsp * piece
+    stack = count // per_dev
+    xs[...] = dot(sort_rows[...], gbuf[...].reshape(count, width)).astype(BF16)
+
+    @pl.loop(0, per_dev)
+    def _(e):
+        for c in weight_copies(e):
+            c.wait()
+        at = pl.ds(pl.multiple_of(e * stack, stack), stack)
+        x = xs[at, :]
+        g = dot(x, eg_v[e])
+        u = dot(x, eu_v[e])
+        h = (g / (1.0 + jnp.exp(-g)) * u).astype(BF16)
+        ys[at, :] = dot(h, ed_v[e]).astype(BF16)
+
+    def ep_copy(k):
+        return remote(ep_out.at[k], ep_in.at[k], ep_send.at[k], ep_recv.at[k], "tp", mate)
+
+    def ex_copy(k):
+        to = 2 * ((pair + k) % half) + core
+        return remote(
+            ex_out.at[k - 1], ex_in.at[k - 1], ex_send.at[k - 1], ex_recv.at[k - 1], "tp", to
+        )
+
+    turn = list(range(1, half)) + [0]
+    for k in turn:
+        i = (pair + k) % half
+        ep_out[k] = dot(unsort_rows[2 * i + 1 - core], ys[...]).astype(BF16)
+        ep_copy(k).start()
+    for k in turn:
+        i = (pair + k) % half
+        z = dot(unsort_rows[2 * i + core], ys[...])
+        ep_copy(k).wait_recv()
+        z = z + ep_in[k].astype(F32)
+        if k:
+            ex_out[k - 1] = z.astype(BF16)
+            ex_copy(k).start()
+    for k in range(1, half):
+        ex_copy(k).wait_recv()
+        z = z + ex_in[k - 1].astype(F32)
+    z = z.astype(BF16)
+    for s in range(nsp):
+        fin[s] = z[s * piece : (s + 1) * piece]
+
+    def r_copy(k):
+        to = (sp + k) % nsp
+        return remote(fin.at[to], ret.at[sp], r_send.at[k - 1], r_recv.at[sp], "sp", to)
+
+    def r_arrival(k):
+        s = (sp + k) % nsp
+        return remote(fin.at[s], ret.at[s], r_send.at[k - 1], r_recv.at[s], "sp", s)
+
+    for k in order:
+        r_copy(k).start()
+    ret[sp] = fin[sp]
+    factor = jnp.zeros((rows, slots), F32)
+    for k in range(TOP):
+        factor = factor + choose[k] * rw[:, k : k + 1]
+    high = factor.astype(BF16)
+    low = (factor - high.astype(F32)).astype(BF16)
+    for k in range(1, nsp):
+        r_arrival(k).wait_recv()
+    back_rows = ret[...].reshape(slots, width)
+    ffn = dot(high, back_rows) + dot(low, back_rows)
+    out[...] = norm(RESIDUAL_SCALE * hidden.astype(F32) + ffn, gain[1:2, :]).astype(BF16)
+
+    for back in (0, 1):
+        place = nsp - 1 - sp if back else sp
+
+        @pl.when(place < nsp - 1)
+        def _():
+            chain_copy_b(back).wait_send()
+            for c in range(chunks):
+                chain_copy(back, c).wait_send()
+
+    for n in range(tiles):
+        p_copy(n).wait_send()
+        for k in range(1, half):
+            x_copy(n, k).wait_send()
+    for k in range(1, nsp):
+        d_copy(k).wait_send()
+        r_copy(k).wait_send()
+    for k in range(nsp):
+        for which in range(2 * half - 1):
+            g_copy(tp, sp, mate, which, k).wait_send()
+    for k in range(half):
+        ep_copy(k).wait_send()
+    for k in range(1, half):
+        ex_copy(k).wait_send()
+
+
+def fits(mesh_sizes, heads_b, width_b, experts_here, rows):
+    nsp, ntp = mesh_sizes
+    aligned = (experts_here * CAP) % 16 == 0 and rows % 16 == 0 and heads_b * 64 % 128 == 0
+    return ntp % 2 == 0 and ntp >= 4 and nsp >= 2 and aligned
+
+
+def fused(
+    query_a,
+    key_a,
+    value_a,
+    decay_a,
+    query_b,
+    key_b,
+    value_b,
+    decay_b,
+    out_weight_a,
+    out_weight_b,
+    residual,
+    norm_gain,
+    route_group,
+    route_expert,
+    route_weight,
+    expert_gate,
+    expert_up,
+    expert_down,
+):
+    nsp, ntp = lax.axis_size("sp"), lax.axis_size("tp")
+    length = query_a.shape[0]
+    rows, width = residual.shape
+    ha, hb = decay_a.shape[1], decay_b.shape[1]
+    dka, dva = query_a.shape[1] // ha, value_a.shape[1] // ha
+    dkb, wb = query_b.shape[1] // hb, query_b.shape[1]
+    per_dev, _, ff = expert_gate.shape
+    piece = per_dev * CAP
+    half = ntp // 2
+    chunks = ha * dva // LANES
+    heads = 2 * (ha + hb)
+    dec = jnp.concatenate([decay_a.reshape(2 * ha, length), decay_b.reshape(2 * hb, length)])
+    positions = (lax.axis_index("sp") * length + jnp.arange(length, dtype=jnp.int32)).astype(F32)
+
+    def angles(hw):
+        freq = ROPE_BASE ** (-jnp.arange(hw, dtype=F32) / hw)
+        return positions[:, None] * freq[None, :]
+
+    ang_a = angles(dka // 2)
+    ang_b = angles(dkb // 2)
+    cos_b, sin_b = jnp.cos(ang_b), jnp.sin(ang_b)
+    cos_b = jnp.tile(cos_b, (1, 2 * hb))
+    sin_b = jnp.tile(sin_b, (1, 2 * hb))
+    lane = np.arange(wb)
+    head_mask = (lane[None, :] // dkb == np.arange(hb)[:, None]).astype(np.float32)
+    block_mask = (lane[None, :] // dkb == lane[:, None] // dkb).astype(np.float32)
+    first = lane % dkb < dkb // 2
+    perm = np.zeros((wb, wb), np.float32)
+    perm[np.where(first, lane + dkb // 2, lane - dkb // 2), lane] = np.where(first, -1.0, 1.0)
+    count = ntp * nsp * piece
+    o = np.arange(count)
+    stack = count // per_dev
+    source = (o % stack) // CAP * piece + o // stack * CAP + o % CAP
+    sort_rows = np.zeros((count, count), np.float32)
+    sort_rows[o, source] = 1.0
+    unsort_rows = sort_rows.T.reshape(ntp, nsp * piece, count)
+    tiles = 4 if width % 512 == 0 else 1
+    tile = width // tiles
+    vmem = pl.BlockSpec(memory_space=pltpu.VMEM)
+    hbm = pl.BlockSpec(memory_space=pl.ANY)
+    dma = pltpu.SemaphoreType.DMA
+    V = pltpu.VMEM
+    return pl.pallas_call(
+        functools.partial(layer_kernel, {"nsp": nsp, "ntp": ntp, "ha": ha, "hb": hb}),
+        out_shape=jax.ShapeDtypeStruct((rows, width), BF16),
+        in_specs=[vmem] * 16 + [hbm] * 2 + [vmem] * 5 + [hbm] * 3,
+        out_specs=vmem,
+        scratch_shapes=[
+            V((out_weight_a.shape[0] + out_weight_b.shape[0], width), BF16),
+            V(expert_gate.shape, BF16),
+            V(expert_up.shape, BF16),
+            V(expert_down.shape, BF16),
+            V((length, ha * dka), BF16),
+            V((length, ha * dka), BF16),
+            V((length, wb), BF16),
+            V((length, wb), BF16),
+            V((length, ha * dva), F32),
+            V((length, wb), F32),
+            V((length, ha * dva + wb), BF16),
+            V((2, chunks, dka, LANES), F32),
+            V((2, dkb, wb), F32),
+            V((2, chunks, 8, LANES), F32),
+            V((2, 8, wb), F32),
+            V((2, chunks, dka, LANES), BF16),
+            V((2, dkb, wb), BF16),
+            V((2, chunks, dka, LANES), BF16),
+            V((2, dkb, wb), BF16),
+            V((tiles, half * rows, tile), BF16),
+            V((tiles, half * rows, tile), BF16),
+            V((half - 1, tiles, rows, tile), BF16),
+            V((half - 1, tiles, rows, tile), BF16),
+            V((tiles, half * rows, tile), F32),
+            V((ntp, nsp, piece, width), BF16),
+            V((nsp, piece, width), BF16),
+            V((count, width), BF16),
+            V((count, width), BF16),
+            V((half, nsp * piece, width), BF16),
+            V((half, nsp * piece, width), BF16),
+            V((half - 1, nsp * piece, width), BF16),
+            V((half - 1, nsp * piece, width), BF16),
+            V((nsp, piece, width), BF16),
+            V((nsp, piece, width), BF16),
+            dma((3, per_dev)),
+            dma((2,)),
+            dma((2, chunks)),
+            dma((2, chunks)),
+            dma((2,)),
+            dma((2,)),
+            dma((tiles,)),
+            dma((tiles,)),
+            dma((half - 1, tiles)),
+            dma((half - 1, tiles)),
+            dma((nsp - 1,)),
+            dma((2 * half - 1, nsp)),
+            dma((ntp, nsp)),
+            dma((half,)),
+            dma((half,)),
+            dma((half - 1,)),
+            dma((half - 1,)),
+            dma((nsp - 1,)),
+            dma((nsp,)),
+        ],
+        compiler_params=pltpu.CompilerParams(
+            collective_id=0, has_side_effects=True, vmem_limit_bytes=60 * 1024 * 1024
+        ),
+    )(
+        query_a,
+        key_a,
+        value_a,
+        query_b,
+        key_b,
+        value_b,
+        dec,
+        jnp.cos(ang_a),
+        jnp.sin(ang_a),
+        cos_b,
+        sin_b,
+        jnp.asarray(head_mask),
+        jnp.asarray(block_mask),
+        jnp.asarray(perm, BF16),
+        jnp.asarray(sort_rows, BF16),
+        jnp.asarray(unsort_rows, BF16),
+        out_weight_a,
+        out_weight_b,
+        residual,
+        norm_gain,
+        route_group[:, None],
+        route_expert,
+        route_weight,
+        expert_gate,
+        expert_up,
+        expert_down,
+    )
+
+
+def layer(*args):
+    sizes = (lax.axis_size("sp"), lax.axis_size("tp"))
+    heads_b, experts_here, rows = args[7].shape[1], args[15].shape[0], args[10].shape[0]
+    if fits(sizes, heads_b, args[4].shape[1], experts_here, rows):
+        return fused(*args)
+    return shards(*args)
+
+
 def solution(mesh):
     return jax.shard_map(
-        shards,
+        layer,
         mesh=mesh,
         in_specs=(
             P(("grp", "sp"), "tp"),

time: 344 us -> 98.1 us (0.29)
  Pallas kernels: 0 us -> 86.9 us
  local copies, waits for them, and re-layouts: 84.7 us -> 8.86 us
  waiting for transfers between devices: 75.7 us -> 0 us
  blocking collectives: 60.1 us -> 0 us
  matrix products: 60 us -> 0 us
  other arithmetic: 40.3 us -> 2.05 us
  between operations: 15 us -> 0.03 us
  starting transfers between devices: 4.99 us -> 0 us
    pallas_call x0 -> x1, Pallas kernels: none -> 86.9 us  [fused(): pl.pallas_call(functools.partial(layer_kernel, {'nsp': nsp, 'ntp': ntp, '...]
    dot_general x33 -> x0, matrix products: 60 us -> none  [the longest x8 15.6 us: advance(): jnp.einsum('ihd,hdv->ihv', query_blk.astype(jnp.float32), state_now, prec...]
    reduce_scatter x2 -> x0, waiting for transfers between devices: 52.4 us -> none  [the longest x1 27.6 us: shards(): lax.psum_scatter((jnp.dot(mixed_a, out_weight_a, preferred_element_type=j...]
    all_gather x2 -> x0, blocking collectives: 35.1 us -> none  [entering(): lax.all_gather(a.astype(kind), axis)]
    dynamic_update_slice x12 -> x0, local copies, waits for them, and re-layouts: 25.6 us -> none  [sweep_blocks(): lax.scan(advance, state_init, (split_blocks(queries), split_blocks(keys_r...]
    rev x13 -> x0, local copies, waits for them, and re-layouts: 17.2 us -> none  [the longest x2 9.85 us: finish(): total_sum = forward + backward_flipped[::-1]]
    all_gather x3 -> x0, waiting for transfers between devices: 14.7 us -> none  [the longest x1 14.7 us: shards(): piece_rows = lax.all_gather(received, 'tp', axis=0, tiled=True)]
    all_to_all x1 -> x0, blocking collectives: 13.2 us -> none  [shards(): lax.all_to_all(outgoing, 'sp', split_axis=0, concat_axis=0, tiled=True)]
  transfers between devices with their start and end apart: 6 -> 0, of which waited for: 4 -> 0; matrix products, arithmetic and copies ran while one was open for 18% -> 0% of each run, Pallas kernels for 0% -> 0%
where the time goes in v1:
time: 98.1 us; the launch traced here: 97.9 us
  Pallas kernels  86.9 us (89%)
  local copies, waits for them, and re-layouts  8.86 us (9%)
  other arithmetic  2.05 us (2%)
    pallas_call x1, Pallas kernels, fused(): pl.pallas_call(functools.partial(layer_kernel, {'nsp': nsp, 'ntp': ntp, '...  86.9 us
    unnamed x3, local copies, waits for them, and re-layouts  4.41 us

profile of v1, /device:TPU:0, one launch (start us, length us, event | category | flops | bytes accessed | tf_op | source)
XLA Modules:
  0.0 97.9 jit_solution(13645408903379298478)
XLA Ops:
  0.0 0.7 reshape.82
  0.7 0.7 reshape.83
  1.4 0.6 pad_maximum_fusion.dec
  2.0 1.3 %copy.29.rg = s32[64,1]{1,0:T(8,128)} copy(s32[64,1]{0,1:T(1,128)} %bitcast.5) | data formatting | bytes 512 | tf_op jit(solution)/shard_map/broadcast_in_dim | solution.py:986
  3.4 1.4 %copy.30.re = s32[64,2]{1,0:T(8,128)} copy(s32[64,2]{0,1:T(2,128)} %param.36) | data formatting | bytes 1024 | tf_op args[13]
  4.8 1.4 %copy.31.rw = f32[64,2]{1,0:T(8,128)} copy(f32[64,2]{0,1:T(2,128)} %param.37) | data formatting | bytes 1024 | tf_op args[14]
  6.1 0.2 multiply_sine_fusion.1
  6.3 0.8 copy.28.sin_b
  7.2 1.2 %multiply_sine_fusion = (f32[256,128]{1,0:T(8,128)}, f32[256,128]{1,0:T(8,128)}) fusion(f32[128]{0:T(128)S(1)} %multiply_power_fusion.1, f32[256]{0:T(256)S(1)} %add_convert_fusion), kind=kLoop, calls=%fused_computation | loop fusion | flops 32768 | bytes 263680 | tf_op jit(solution)/shard_map/sin | solution.py:974
  8.4 0.8 copy.27.cos_b
  9.3 86.9 %shard_map.217 = bf16[64,2048]{1,0:T(8,128)(2,1)} custom-call(bf16[256,512]{1,0:T(8,128)(2,1)} %qa.1, bf16[256,512]{1,0:T(8,128)(2,1)} %ka.1, bf16[256,1024]{1,0:T(8,128)(2,1)} %va.1, bf16[256,256]{1,0:T(8,128)(2,1)} %qb.1, bf16[256,256]{1,0:T(8,128)(2,1)} %kb.1, bf16[256,256]{1,0:T(8,128)(2,1)} %vb.1, f32[12,256]{1,0:T(8,128)} %pad_maximum_fusion.dec, ...), custom_call_target="tpu_custom_call" | custom-call | tf_op jit(solution)/shard_map/pallas_call | solution.py:902
  96.2 1.7 %copy.33 = bf16[64,2048]{1,0:T(8,128)(2,1)} copy(bf16[64,2048]{1,0:T(8,128)(2,1)} %shard_map.217) | data formatting | bytes 524288
  (5 shorter events, 0.1 us)

commit v2 on v1

--- a/solution.py
+++ b/solution.py
@@ -312,11 +312,14 @@
     qb,
     kb,
     vb,
-    dec,
+    dec_a,
+    dec_b,
     cos_a,
     sin_a,
     cos_b,
     sin_b,
+    start_a,
+    start_b,
     head_mask,
     block_mask,
     rope_perm,
@@ -333,6 +336,7 @@
     eu,
     ed,
     out,
+    dec,
     wo_v,
     eg_v,
     eu_v,
@@ -360,7 +364,9 @@
     gbuf,
     obuf,
     xs,
+    hs,
     ys,
+    eown,
     ep_out,
     ep_in,
     ex_out,
@@ -446,6 +452,9 @@
     lower = r_i >= c_i
     tri = jnp.where(lower, 1.0, 0.0).astype(F32)
     tri_s = jnp.where(r_i > c_i, 1.0, 0.0).astype(F32)
+    for back in (0, 1):
+        dec[back * ha : (back + 1) * ha] = dec_a[back]
+        dec[2 * ha + back * hb : 2 * ha + (back + 1) * hb] = dec_b[back]
     d = dec[...]
     inc_col = dot(tri, d, NT, HIGHEST)
     inc_row = dot(d, tri, NT, HIGHEST)
@@ -469,7 +478,13 @@
         return arr[i : i + 1, :]
 
     hw = dka // 2
-    ca, sa = cos_a[...], sin_a[...]
+
+    def turned(start, cosine, sine):
+        sc, ss = start[sp, 0:1], start[sp, 1:2]
+        return sc * cosine[...] - ss * sine[...], ss * cosine[...] + sc * sine[...]
+
+    ca, sa = turned(start_a, cos_a, sin_a)
+    cb, sb = turned(start_b, cos_b, sin_b)
 
     def rot_a(x, scale):
         x1, x2 = x[:, :hw].astype(F32), x[:, hw:].astype(F32)
@@ -481,28 +496,59 @@
     vbv = vb[...]
 
     def rot_b(x, scale):
-        y = x.astype(F32) * cos_b[...] + dot(x, rope_perm[...]) * sin_b[...]
+        y = x.astype(F32) * cb + dot(x, rope_perm[...]) * sb
         return (y * scale).astype(BF16)
 
     def spread(cols):
         return functools.reduce(lambda x, y: x + y, [c * m for c, m in zip(cols, masks)])
 
-    kbr = rot_b(kb[...], 1.0 / math.sqrt(dkb))
-    kb_s[...] = kbr
-    for back in (0, 1):
-        if back:
-            scale = spread([jnp.exp(col(exc_col, "b", 1, j)) for j in range(hb)])
-        else:
-            scale = spread(
-                [jnp.exp(tot("b", 0, j) - col(inc_col, "b", 0, j)) for j in range(hb)]
-            )
-        full = dot((kbr.astype(F32) * scale).astype(BF16), vbv, TN) * bm
-        loc_b[back] = functools.reduce(
-            lambda x, y: x + y, [full[j * dkb : (j + 1) * dkb] for j in range(hb)]
-        )
-        dfs_b[back] = jnp.broadcast_to(
-            spread([jnp.exp(tot("b", back, j)) for j in range(hb)]), dfs_b.shape[1:]
-        )
+    pl.semaphore_wait(barrier, nsp - 1 + ntp - 1)
+
+    @pl.when(sp == 0)
+    def _():
+        cin[0] = jnp.zeros(cin.shape[1:], BF16)
+        cin_b[0] = jnp.zeros(cin_b.shape[1:], BF16)
+
+    @pl.when(sp == nsp - 1)
+    def _():
+        cin[1] = jnp.zeros(cin.shape[1:], BF16)
+        cin_b[1] = jnp.zeros(cin_b.shape[1:], BF16)
+
+    def chain_copy(back, c):
+        to = (sp + nsp - 1) % nsp if back else (sp + 1) % nsp
+        return remote(
+            cout.at[back, c], cin.at[back, c], c_send.at[back, c], c_recv.at[back, c], "sp", to
+        )
+
+    def chain_copy_b(back):
+        to = (sp + nsp - 1) % nsp if back else (sp + 1) % nsp
+        return remote(
+            cout_b.at[back], cin_b.at[back], cb_send.at[back], cb_recv.at[back], "sp", to
+        )
+
+    def place_of(back):
+        return nsp - 1 - sp if back else sp
+
+    def chain(back, t):
+        place = place_of(back)
+        c = t - 2 * (place - 1)
+
+        @pl.when((place > 0) & (place < nsp - 1) & (c >= 0) & (c < chunks))
+        def _():
+            chain_copy(back, c).wait_recv()
+            cout[back, c] = (
+                cin[back, c].astype(F32) * dfs[back, c][:1] + loc[back, c]
+            ).astype(BF16)
+            chain_copy(back, c).start()
+
+        @pl.when((place > 0) & (place < nsp - 1) & (c == chunks - 1))
+        def _():
+            chain_copy_b(back).wait_recv()
+            cout_b[back] = (
+                cin_b[back].astype(F32) * dfs_b[back][:1] + loc_b[back]
+            ).astype(BF16)
+            chain_copy_b(back).start()
+
     for h in range(ha):
         k = rot_a(ka[:, h * dka : (h + 1) * dka], 1.0 / math.sqrt(dka))
         ka_s[:, h * dka : (h + 1) * dka] = k
@@ -519,59 +565,33 @@
                     jnp.exp(tot("a", back, h)), dfs.shape[2:]
                 )
 
-    pl.semaphore_wait(barrier, nsp - 1 + ntp - 1)
-
-    @pl.when(sp == 0)
-    def _():
-        cin[0] = jnp.zeros(cin.shape[1:], BF16)
-        cin_b[0] = jnp.zeros(cin_b.shape[1:], BF16)
-
-    @pl.when(sp == nsp - 1)
-    def _():
-        cin[1] = jnp.zeros(cin.shape[1:], BF16)
-        cin_b[1] = jnp.zeros(cin_b.shape[1:], BF16)
-
-    def chain_copy(back, c):
-        to = (sp + nsp - 1) % nsp if back else (sp + 1) % nsp
-        return remote(
-            cout.at[back, c], cin.at[back, c], c_send.at[back, c], c_recv.at[back, c], "sp", to
-        )
-
-    def chain_copy_b(back):
-        to = (sp + nsp - 1) % nsp if back else (sp + 1) % nsp
-        return remote(
-            cout_b.at[back], cin_b.at[back], cb_send.at[back], cb_recv.at[back], "sp", to
-        )
-
-    def chain(back, t):
-        place = nsp - 1 - sp if back else sp
-        c = t - place
-
-        @pl.when((c >= 0) & (c < chunks))
+            @pl.when(place_of(back) == 0)
+            def _():
+                for c in range(h * cph, (h + 1) * cph):
+                    cout[back, c] = loc[back, c].astype(BF16)
+                    chain_copy(back, c).start()
+
+    kbr = rot_b(kb[...], 1.0 / math.sqrt(dkb))
+    kb_s[...] = kbr
+    for back in (0, 1):
+        if back:
+            scale = spread([jnp.exp(col(exc_col, "b", 1, j)) for j in range(hb)])
+        else:
+            scale = spread(
+                [jnp.exp(tot("b", 0, j) - col(inc_col, "b", 0, j)) for j in range(hb)]
+            )
+        full = dot((kbr.astype(F32) * scale).astype(BF16), vbv, TN) * bm
+        loc_b[back] = functools.reduce(
+            lambda x, y: x + y, [full[j * dkb : (j + 1) * dkb] for j in range(hb)]
+        )
+        dfs_b[back] = jnp.broadcast_to(
+            spread([jnp.exp(tot("b", back, j)) for j in range(hb)]), dfs_b.shape[1:]
+        )
+
+        @pl.when(place_of(back) == 0)
         def _():
-            @pl.when(place > 0)
-            def _():
-                chain_copy(back, c).wait_recv()
-
-            @pl.when(place < nsp - 1)
-            def _():
-                cout[back, c] = (
-                    cin[back, c].astype(F32) * dfs[back, c][:1] + loc[back, c]
-                ).astype(BF16)
-                chain_copy(back, c).start()
-
-        @pl.when(c == 0)
-        def _():
-            @pl.when(place > 0)
-            def _():
-                chain_copy_b(back).wait_recv()
-
-            @pl.when(place < nsp - 1)
-            def _():
-                cout_b[back] = (
-                    cin_b[back].astype(F32) * dfs_b[back][:1] + loc_b[back]
-                ).astype(BF16)
-                chain_copy_b(back).start()
+            cout_b[back] = loc_b[back].astype(BF16)
+            chain_copy_b(back).start()
 
     def weights(kind, h):
         ahead = col(inc_col, kind, 0, h) - row(inc_row, kind, 0, h)
@@ -599,7 +619,8 @@
 
     work = [functools.partial(local_a, h) for h in range(ha)]
     work += [functools.partial(local_b, j) for j in range(hb)]
-    steps = chunks + nsp - 1
+    steps = chunks + 2 * max(nsp - 3, 0)
+    work.pop(0)()
     for t in range(steps):
         chain(0, t)
         chain(1, t)
@@ -607,6 +628,14 @@
             work[t]()
     for piece in work[steps:]:
         piece()
+    for back in (0, 1):
+
+        @pl.when(place_of(back) == nsp - 1)
+        def _():
+            for c in range(chunks):
+                chain_copy(back, c).wait_recv()
+            chain_copy_b(back).wait_recv()
+
 
     for h in range(ha):
         q = qa_s[:, h * dka : (h + 1) * dka]
@@ -682,25 +711,30 @@
     hidden = norm(RESIDUAL_SCALE * res[...].astype(F32) + mix, gain[0:1, :]).astype(BF16)
 
     slots = EXPERTS * CAP
-    lane_e = lax.broadcasted_iota(jnp.int32, (rows, EXPERTS), 1)
-    lane_s = lax.broadcasted_iota(jnp.int32, (rows, slots), 1)
-    ids = [rg[...] * EXP_GROUP + re[:, k : k + 1] for k in range(TOP)]
-    hot = [jnp.where(i == lane_e, 1.0, 0.0) for i in ids]
+    line_e = lax.broadcasted_iota(jnp.int32, (EXPERTS, rows), 0)
+    line_s = lax.broadcasted_iota(jnp.int32, (slots, rows), 0)
+    ids = [rg[...] * EXP_GROUP + re[k : k + 1, :] for k in range(TOP)]
+    hot = [jnp.where(i == line_e, 1.0, 0.0) for i in ids]
     before = jnp.where(
         lax.broadcasted_iota(jnp.int32, (rows, rows), 0)
-        > lax.broadcasted_iota(jnp.int32, (rows, rows), 1),
+        < lax.broadcasted_iota(jnp.int32, (rows, rows), 1),
         1.0,
         0.0,
     )
-    earlier = dot(before.astype(BF16), functools.reduce(jnp.add, hot).astype(BF16))
+    earlier = dot(functools.reduce(jnp.add, hot).astype(BF16), before.astype(BF16))
     choose = []
     for i, o in zip(ids, hot):
-        rank = jnp.sum(earlier * o, axis=1, keepdims=True)
-        hit = jnp.zeros((rows, slots), F32)
+        rank = jnp.sum(earlier * o, axis=0, keepdims=True)
+        hit = jnp.zeros((slots, rows), F32)
         for c in range(CAP):
-            hit = hit + jnp.where((lane_s == i * CAP + c) & (rank == float(c)), 1.0, 0.0)
+            hit = hit + jnp.where((line_s == i * CAP + c) & (rank == float(c)), 1.0, 0.0)
         choose.append(hit)
-    outgoing = dot(functools.reduce(jnp.add, choose).astype(BF16), hidden, TN).astype(BF16)
+    factor = jnp.zeros((slots, rows), F32)
+    for k in range(TOP):
+        factor = factor + choose[k] * rw[k : k + 1, :]
+    high = factor.astype(BF16)
+    low = (factor - high.astype(F32)).astype(BF16)
+    outgoing = dot(functools.reduce(jnp.add, choose).astype(BF16), hidden).astype(BF16)
     piece = per_dev * CAP
     for s in range(nsp):
         obuf[s] = outgoing[s * piece : (s + 1) * piece]
@@ -753,57 +787,78 @@
         g = dot(x, eg_v[e])
         u = dot(x, eu_v[e])
         h = (g / (1.0 + jnp.exp(-g)) * u).astype(BF16)
-        ys[at, :] = dot(h, ed_v[e]).astype(BF16)
-
-    def ep_copy(k):
-        return remote(ep_out.at[k], ep_in.at[k], ep_send.at[k], ep_recv.at[k], "tp", mate)
-
-    def ex_copy(k):
+        hs[at, :] = h
+
+    def ep_copy(n):
+        return remote(ep_out.at[n], ep_in.at[n], ep_send.at[n], ep_recv.at[n], "tp", mate)
+
+    def ex_copy(n, k):
         to = 2 * ((pair + k) % half) + core
         return remote(
-            ex_out.at[k - 1], ex_in.at[k - 1], ex_send.at[k - 1], ex_recv.at[k - 1], "tp", to
-        )
-
-    turn = list(range(1, half)) + [0]
-    for k in turn:
-        i = (pair + k) % half
-        ep_out[k] = dot(unsort_rows[2 * i + 1 - core], ys[...]).astype(BF16)
-        ep_copy(k).start()
-    for k in turn:
-        i = (pair + k) % half
-        z = dot(unsort_rows[2 * i + core], ys[...])
-        ep_copy(k).wait_recv()
-        z = z + ep_in[k].astype(F32)
-        if k:
-            ex_out[k - 1] = z.astype(BF16)
-            ex_copy(k).start()
-    for k in range(1, half):
-        ex_copy(k).wait_recv()
-        z = z + ex_in[k - 1].astype(F32)
-    z = z.astype(BF16)
-    for s in range(nsp):
-        fin[s] = z[s * piece : (s + 1) * piece]
-
-    def r_copy(k):
+            ex_out.at[k - 1, n],
+            ex_in.at[k - 1, n],
+            ex_send.at[k - 1, n],
+            ex_recv.at[k - 1, n],
+            "tp",
+            to,
+        )
+
+    def r_copy(n, k):
         to = (sp + k) % nsp
-        return remote(fin.at[to], ret.at[sp], r_send.at[k - 1], r_recv.at[sp], "sp", to)
-
-    def r_arrival(k):
+        return remote(
+            fin.at[n, to], ret.at[n, sp], r_send.at[n, k - 1], r_recv.at[n, sp], "sp", to
+        )
+
+    def r_arrival(n, k):
         s = (sp + k) % nsp
-        return remote(fin.at[s], ret.at[s], r_send.at[k - 1], r_recv.at[s], "sp", s)
-
-    for k in order:
-        r_copy(k).start()
-    ret[sp] = fin[sp]
-    factor = jnp.zeros((rows, slots), F32)
-    for k in range(TOP):
-        factor = factor + choose[k] * rw[:, k : k + 1]
-    high = factor.astype(BF16)
-    low = (factor - high.astype(F32)).astype(BF16)
-    for k in range(1, nsp):
-        r_arrival(k).wait_recv()
-    back_rows = ret[...].reshape(slots, width)
-    ffn = dot(high, back_rows) + dot(low, back_rows)
+        return remote(fin.at[n, s], ret.at[n, s], r_send.at[n, k - 1], r_recv.at[n, s], "sp", s)
+
+    group = nsp * piece
+    turn = [(pair + k) % half for k in range(half)]
+    to_mate = jnp.concatenate([unsort_rows[2 * i + 1 - core] for i in turn], axis=0)
+    to_own = jnp.concatenate([unsort_rows[2 * i + core] for i in turn], axis=0)
+
+    def down(n):
+        for e in range(per_dev):
+            y = dot(hs[e * stack : (e + 1) * stack, :], ed_v[e, :, n * tile : (n + 1) * tile])
+            ys[e * stack : (e + 1) * stack, :] = y.astype(BF16)
+        ep_out[n] = dot(to_mate, ys[...]).astype(BF16)
+        ep_copy(n).start()
+        eown[n] = dot(to_own, ys[...])
+
+    def across(n):
+        ep_copy(n).wait_recv()
+        eown[n] += ep_in[n].astype(F32)
+        for k in range(1, half):
+            ex_out[k - 1, n] = eown[n, k * group : (k + 1) * group, :].astype(BF16)
+            ex_copy(n, k).start()
+
+    def home(n):
+        z = eown[n, :group, :]
+        for k in range(1, half):
+            ex_copy(n, k).wait_recv()
+            z = z + ex_in[k - 1, n].astype(F32)
+        z = z.astype(BF16)
+        for s in range(nsp):
+            fin[n, s] = z[s * piece : (s + 1) * piece]
+        for k in order:
+            r_copy(n, k).start()
+        ret[n, sp] = fin[n, sp]
+
+    for i in range(tiles + 3):
+        if i < tiles:
+            down(i)
+        if 0 <= i - 1 < tiles:
+            across(i - 1)
+        if 0 <= i - 3 < tiles:
+            home(i - 3)
+    ffn = []
+    for n in range(tiles):
+        for k in range(1, nsp):
+            r_arrival(n, k).wait_recv()
+        back_rows = ret[n].reshape(slots, tile)
+        ffn.append(dot(high, back_rows, TN) + dot(low, back_rows, TN))
+    ffn = jnp.concatenate(ffn, axis=1)
     out[...] = norm(RESIDUAL_SCALE * hidden.astype(F32) + ffn, gain[1:2, :]).astype(BF16)
 
     for back in (0, 1):
@@ -821,14 +876,15 @@
             x_copy(n, k).wait_send()
     for k in range(1, nsp):
         d_copy(k).wait_send()
-        r_copy(k).wait_send()
+        for n in range(tiles):
+            r_copy(n, k).wait_send()
     for k in range(nsp):
         for which in range(2 * half - 1):
             g_copy(tp, sp, mate, which, k).wait_send()
-    for k in range(half):
-        ep_copy(k).wait_send()
-    for k in range(1, half):
-        ex_copy(k).wait_send()
+    for n in range(tiles):
+        ep_copy(n).wait_send()
+        for k in range(1, half):
+            ex_copy(n, k).wait_send()
 
 
 def fits(mesh_sizes, heads_b, width_b, experts_here, rows):
@@ -868,18 +924,15 @@
     half = ntp // 2
     chunks = ha * dva // LANES
     heads = 2 * (ha + hb)
-    dec = jnp.concatenate([decay_a.reshape(2 * ha, length), decay_b.reshape(2 * hb, length)])
-    positions = (lax.axis_index("sp") * length + jnp.arange(length, dtype=jnp.int32)).astype(F32)
-
-    def angles(hw):
-        freq = ROPE_BASE ** (-jnp.arange(hw, dtype=F32) / hw)
-        return positions[:, None] * freq[None, :]
-
-    ang_a = angles(dka // 2)
-    ang_b = angles(dkb // 2)
-    cos_b, sin_b = jnp.cos(ang_b), jnp.sin(ang_b)
-    cos_b = jnp.tile(cos_b, (1, 2 * hb))
-    sin_b = jnp.tile(sin_b, (1, 2 * hb))
+    def tables(hw, copies):
+        freq = ROPE_BASE ** (-np.arange(hw) / hw)
+        inner = np.tile(np.arange(length)[:, None] * freq, (1, copies))
+        start = np.tile((np.arange(nsp) * length)[:, None] * freq, (1, copies))
+        start = np.stack([np.cos(start), np.sin(start)], axis=1)
+        return [jnp.asarray(t, F32) for t in (np.cos(inner), np.sin(inner), start)]
+
+    cos_a, sin_a, start_a = tables(dka // 2, 1)
+    cos_b, sin_b, start_b = tables(dkb // 2, 2 * hb)
     lane = np.arange(wb)
     head_mask = (lane[None, :] // dkb == np.arange(hb)[:, None]).astype(np.float32)
     block_mask = (lane[None, :] // dkb == lane[:, None] // dkb).astype(np.float32)
@@ -902,9 +955,10 @@
     return pl.pallas_call(
         functools.partial(layer_kernel, {"nsp": nsp, "ntp": ntp, "ha": ha, "hb": hb}),
         out_shape=jax.ShapeDtypeStruct((rows, width), BF16),
-        in_specs=[vmem] * 16 + [hbm] * 2 + [vmem] * 5 + [hbm] * 3,
+        in_specs=[vmem] * 19 + [hbm] * 2 + [vmem] * 5 + [hbm] * 3,
         out_specs=vmem,
         scratch_shapes=[
+            V((heads, length), F32),
             V((out_weight_a.shape[0] + out_weight_b.shape[0], width), BF16),
             V(expert_gate.shape, BF16),
             V(expert_up.shape, BF16),
@@ -932,13 +986,15 @@
             V((ntp, nsp, piece, width), BF16),
             V((nsp, piece, width), BF16),
             V((count, width), BF16),
-            V((count, width), BF16),
-            V((half, nsp * piece, width), BF16),
-            V((half, nsp * piece, width), BF16),
-            V((half - 1, nsp * piece, width), BF16),
-            V((half - 1, nsp * piece, width), BF16),
-            V((nsp, piece, width), BF16),
-            V((nsp, piece, width), BF16),
+            V((count, ff), BF16),
+            V((count, tile), BF16),
+            V((tiles, half * nsp * piece, tile), F32),
+            V((tiles, half * nsp * piece, tile), BF16),
+            V((tiles, half * nsp * piece, tile), BF16),
+            V((half - 1, tiles, nsp * piece, tile), BF16),
+            V((half - 1, tiles, nsp * piece, tile), BF16),
+            V((tiles, nsp, piece, tile), BF16),
+            V((tiles, nsp, piece, tile), BF16),
             dma((3, per_dev)),
             dma((2,)),
             dma((2, chunks)),
@@ -952,12 +1008,12 @@
             dma((nsp - 1,)),
             dma((2 * half - 1, nsp)),
             dma((ntp, nsp)),
-            dma((half,)),
-            dma((half,)),
-            dma((half - 1,)),
-            dma((half - 1,)),
-            dma((nsp - 1,)),
-            dma((nsp,)),
+            dma((tiles,)),
+            dma((tiles,)),
+            dma((half - 1, tiles)),
+            dma((half - 1, tiles)),
+            dma((tiles, nsp - 1)),
+            dma((tiles, nsp)),
         ],
         compiler_params=pltpu.CompilerParams(
             collective_id=0, has_side_effects=True, vmem_limit_bytes=60 * 1024 * 1024
@@ -969,11 +1025,14 @@
         query_b,
         key_b,
         value_b,
-        dec,
-        jnp.cos(ang_a),
-        jnp.sin(ang_a),
+        decay_a,
+        decay_b,
+        cos_a,
+        sin_a,
         cos_b,
         sin_b,
+        start_a,
+        start_b,
         jnp.asarray(head_mask),
         jnp.asarray(block_mask),
         jnp.asarray(perm, BF16),
@@ -983,9 +1042,9 @@
         out_weight_b,
         residual,
         norm_gain,
-        route_group[:, None],
-        route_expert,
-        route_weight,
+        route_group[None, :],
+        route_expert.T,
+        route_weight.T,
         expert_gate,
         expert_up,
         expert_down,

time: 98.1 us -> 75.8 us (0.77)
  Pallas kernels: 86.9 us -> 74 us
  local copies, waits for them, and re-layouts: 8.86 us -> 1.67 us
  other arithmetic: 2.05 us -> 0 us
    pallas_call x1, Pallas kernels: 86.9 us -> 74 us  [fused(): pl.pallas_call(functools.partial(layer_kernel, {'nsp': nsp, 'ntp': ntp, '...]
    unnamed x3 -> x1, local copies, waits for them, and re-layouts: 4.41 us -> 1.67 us
    another operation x4 -> x0, local copies, waits for them, and re-layouts: 1.7 us -> none  [the longest x2 0.86 us: fused(): cos_b = jnp.tile(cos_b, (1, 2 * hb))]
    sin x2 -> x0, other arithmetic: 1.42 us -> none  [the longest x1 1.22 us: fused(): jnp.sin(ang_a)]
    reshape x2 -> x0, local copies, waits for them, and re-layouts: 1.41 us -> none  [the longest x1 0.71 us: fused(): decay_a.reshape(2 * ha, length)]
    broadcast_in_dim x1 -> x0, local copies, waits for them, and re-layouts: 1.34 us -> none  [fused(): route_group[:, None]]
where the time goes in v2:
time: 75.8 us; the launch traced here: 75.6 us
  Pallas kernels  74 us (98%)
  local copies, waits for them, and re-layouts  1.67 us (2%)
    pallas_call x1, Pallas kernels, fused(): pl.pallas_call(functools.partial(layer_kernel, {'nsp': nsp, 'ntp': ntp, '...  74 us
    unnamed x1, local copies, waits for them, and re-layouts  1.67 us

profile of v2, /device:TPU:0, one launch (start us, length us, event | category | flops | bytes accessed | tf_op | source)
XLA Modules:
  0.0 75.6 jit_solution(4946451247494391395)
XLA Ops:
  0.0 74.0 %shard_map.271 = bf16[64,2048]{1,0:T(8,128)(2,1)} custom-call(bf16[256,512]{1,0:T(8,128)(2,1)} %qa.1, bf16[256,512]{1,0:T(8,128)(2,1)} %ka.1, bf16[256,1024]{1,0:T(8,128)(2,1)} %va.1, bf16[256,256]{1,0:T(8,128)(2,1)} %qb.1, bf16[256,256]{1,0:T(8,128)(2,1)} %kb.1, bf16[256,256]{1,0:T(8,128)(2,1)} %vb.1, f32[2,2,256]{2,1,0:T(2,128)} %dec_a.1, ...), custom_call_target="tpu_custom_call" | custom-call | tf_op jit(solution)/shard_map/pallas_call | solution.py:955
  74.0 1.7 %copy.31 = bf16[64,2048]{1,0:T(8,128)(2,1)} copy(bf16[64,2048]{1,0:T(8,128)(2,1)} %shard_map.271) | data formatting | bytes 524288
